TPU v7x, 512 devices: a whole 4x4x16 slice. The times are simulated.
512 devices in a mesh: ep: 32 (over z, core), tp: 16 (over y, x).
Axes of the slice: x: 4, y: 4, z: 16, core: 2. Of those that a mesh axis runs over, the one named last changes fastest.
Arguments:
- query_vectors: bfloat16 [16384, 4096], P('ep', 'tp'), may hold values from -6 to 6
- key_vectors: bfloat16 [16384, 2048], P('ep', 'tp'), may hold values from -6 to 6
- value_vectors: bfloat16 [16384, 2048], P('ep', 'tp'), may hold values from -64 to 64
- query_gain: float32 [128], replicated, may hold values from 0.1 to 1.9
- key_gain: float32 [128], replicated, may hold values from 0.1 to 1.9
- sink_logits: float32 [32], P('tp'), may hold values from 3 to 7
- moe_rows: bfloat16 [5120, 4096], P('ep', 'tp'), may hold values from -6 to 6
- norm_gain: float32 [4096], replicated, may hold values from 0.1 to 1.9
- expert_ids: int32 [5120, 4], P('ep'), may hold values from 0 to 31, all different within a row; in each aligned block of 160 rows (0 to 159, 160 to 319, ...) at most 30 rows name the same one
- route_weights: float32 [5120, 4], P('ep'), may hold values from 0.25 to 2.5
- expert_gate: bfloat16 [32, 4096, 2048], P('ep', None, 'tp'), may hold values from -0.09375 to 0.09375
- expert_up: bfloat16 [32, 4096, 2048], P('ep', None, 'tp'), may hold values from -0.09375 to 0.09375
- expert_down: bfloat16 [32, 2048, 4096], P('ep', None, 'tp'), may hold values from -0.125 to 0.125
- shared_gate: bfloat16 [4096, 512], P(None, 'tp'), may hold values from -0.09375 to 0.09375
- shared_up: bfloat16 [4096, 512], P(None, 'tp'), may hold values from -0.09375 to 0.09375
- shared_down: bfloat16 [512, 4096], P(None, 'tp'), may hold values from -0.25 to 0.25
Outputs:
- attended: bfloat16 [16384, 4096], P('ep', 'tp')
- moe_out: bfloat16 [5120, 4096], P('ep', 'tp')
Inputs may be any that keep to these rules, and one draw needn't show every extreme that they name: `expert_ids`: each row names 4 different experts. Within the rows of one index of ep (aligned blocks of 160 rows), no expert is named by more than 30 rows, and in some block one expert is named by exactly 30.
All inputs are finite; a program needn't handle non-finite values.
Results may differ from a plain program's by a relative error of at most 0.0071.
Values may be sent and summed in bfloat16 or wider, within the bound.
A program may use at most 64 MiB of HBM per device.

v0:
```python
import jax
import jax.numpy as jnp
from jax import lax
from jax.sharding import PartitionSpec as P

HEAD_DIM = 128
WINDOW = 128
GRID_W = 64
D = 4096
TOP_K = 4


epsilon = 1e-06
rotary_base = 10000.0


def padded_2(block, sides, width):
    for axis, dim in sides:
        count = lax.axis_size(axis)
        forward = [(i, i + 1) for i in range(count - 1)]
        backward = [(target, source) for source, target in forward]
        low = lax.ppermute(
            lax.slice_in_dim(block, block.shape[dim] - width, None, axis=dim), axis, forward
        )
        high = lax.ppermute(lax.slice_in_dim(block, 0, width, axis=dim), axis, backward)
        block = jnp.concatenate([low, block, high], axis=dim)
    return block


def side_by_side(arrays, axis, dim, along):
    widths = [a.shape[along] for a in arrays]
    both = jnp.concatenate(arrays, axis=along)
    whole = lax.all_gather(both, axis, axis=dim, tiled=True)
    return tuple(jnp.split(whole, [sum(widths[:k]) for k in range(1, len(widths))], axis=along))


def half_turn(halves):
    leading, trailing = jnp.split(halves, 2, axis=-1)
    return jnp.concatenate([-trailing, leading], axis=-1)


def rotate_heads(vectors, head_gain, positions):
    floats = vectors.astype(jnp.float32)
    normed = (
        floats * lax.rsqrt(jnp.mean(floats * floats, axis=-1, keepdims=True) + epsilon) * head_gain
    )
    quarter = HEAD_DIM // 4
    freq_index = jnp.arange(quarter, dtype=jnp.int32).astype(jnp.float32)
    inverse = rotary_base ** (-4.0 * freq_index / HEAD_DIM)
    grid_row = (positions // GRID_W).astype(jnp.float32)[:, None] * inverse
    grid_col = (positions % GRID_W).astype(jnp.float32)[:, None] * inverse
    angles = jnp.concatenate([grid_row, grid_row, grid_col, grid_col], axis=-1)[:, None, :]
    row_half, col_half = jnp.split(normed, 2, axis=-1)
    turned = jnp.concatenate([half_turn(row_half), half_turn(col_half)], axis=-1)
    return (normed * jnp.cos(angles) + turned * jnp.sin(angles)).astype(jnp.bfloat16)


def attend_window(query_vectors, key_vectors, value_vectors, query_gain, key_gain, sink_logits):
    length = query_vectors.shape[0]
    heads_here = sink_logits.shape[0]
    kv_here = key_vectors.shape[1] // HEAD_DIM
    grouping = heads_here // kv_here
    shard_start = lax.axis_index("ep") * length
    positions = shard_start + jnp.arange(length, dtype=jnp.int32)
    queries = rotate_heads(
        query_vectors.reshape(length, heads_here, HEAD_DIM), query_gain, positions
    )
    turned_keys = rotate_heads(key_vectors.reshape(length, kv_here, HEAD_DIM), key_gain, positions)
    turned_keys = turned_keys.reshape(length, kv_here * HEAD_DIM)
    padded = padded_2(jnp.stack([turned_keys, value_vectors]), (("ep", 1),), WINDOW)
    extent = length + 2 * WINDOW
    near_keys = padded[0].reshape(extent, kv_here, HEAD_DIM)
    near_values = padded[1].reshape(extent, kv_here, HEAD_DIM)
    key_pos = shard_start - WINDOW + jnp.arange(extent, dtype=jnp.int32)
    inside = (
        (jnp.abs(positions[:, None] - key_pos[None, :]) <= WINDOW)
        & (key_pos >= 0)[None, :]
        & (key_pos < lax.axis_size("ep") * length)[None, :]
    )
    scores = jnp.einsum(
        "qhgd,khd->hgqk",
        queries.reshape(length, kv_here, grouping, HEAD_DIM),
        near_keys,
        preferred_element_type=jnp.float32,
    ) * HEAD_DIM ** (-0.5)
    raised = jnp.where(inside, jnp.exp(scores), 0.0)
    denominator = jnp.exp(sink_logits).reshape(kv_here, grouping)[:, :, None] + jnp.sum(
        raised, axis=-1
    )
    weights = (raised / denominator[..., None]).astype(jnp.bfloat16)
    mixed = jnp.einsum("hgqk,khd->qhgd", weights, near_values, preferred_element_type=jnp.float32)
    return mixed.astype(jnp.bfloat16).reshape(length, heads_here * HEAD_DIM)


def project(block_rows, gain_piece, gate_rows, up_rows):
    floats = block_rows.astype(jnp.float32)
    weighted = (floats * gain_piece).astype(jnp.bfloat16)
    gate_sum = jnp.dot(weighted, gate_rows, preferred_element_type=jnp.float32)
    up_sum = jnp.dot(weighted, up_rows, preferred_element_type=jnp.float32)
    return (gate_sum, up_sum, jnp.sum(floats * floats, axis=1))


def activate(gate_sum, up_sum, squares):
    factor = lax.rsqrt(squares / D + epsilon)[:, None]
    return (jax.nn.silu(gate_sum * factor) * (up_sum * factor)).astype(jnp.bfloat16)


def shards(
    query_vectors,
    key_vectors,
    value_vectors,
    query_gain,
    key_gain,
    sink_logits,
    moe_rows,
    norm_gain,
    expert_ids,
    route_weights,
    expert_gate,
    expert_up,
    expert_down,
    shared_gate,
    shared_up,
    shared_down,
):
    attended = attend_window(
        query_vectors, key_vectors, value_vectors, query_gain, key_gain, sink_logits
    )
    ep_size = lax.axis_size("ep")
    tokens_here, width_here = moe_rows.shape
    capacity = max(2, 3 * tokens_here * TOP_K // (2 * ep_size))
    slots_all = ep_size * capacity
    flat_ids = expert_ids.reshape(-1)
    onehot = (flat_ids[:, None] == jnp.arange(ep_size, dtype=jnp.int32)[None, :]).astype(jnp.int32)
    slot_index = jnp.sum((jnp.cumsum(onehot, axis=0) - onehot) * onehot, axis=1)
    target = flat_ids * capacity + slot_index
    matches = target[None, :] == jnp.arange(slots_all, dtype=jnp.int32)[:, None]
    present = jnp.any(matches, axis=1)
    owner_row = jnp.arange(tokens_here * TOP_K, dtype=jnp.int32) // TOP_K
    source_row = jnp.sum(jnp.where(matches, owner_row[None, :], 0), axis=1)
    local_gate = expert_gate[0]
    local_up = expert_up[0]
    local_down = expert_down[0]
    units_here = local_gate.shape[1]
    shared_units = shared_gate.shape[1]
    outgoing = jnp.where(
        present[:, None], jnp.take(moe_rows, source_row, axis=0), jnp.zeros((), jnp.bfloat16)
    )
    arrived = lax.all_to_all(
        outgoing.reshape(ep_size, capacity, width_here),
        "ep",
        split_axis=0,
        concat_axis=0,
        tiled=True,
    )
    arrived = arrived.reshape(slots_all, width_here)
    pieces = side_by_side((arrived, moe_rows), "tp", 1, 0)
    routed = project(pieces[0], norm_gain, local_gate, local_up)
    shared = project(pieces[1], norm_gain, shared_gate, shared_up)
    gate_sum, up_sum, squares, shared_gsum, shared_usum, own_squares = tuple(
        (new_term for new_term in routed + shared)
    )
    hidden = activate(gate_sum, up_sum, squares)
    shared_hidden = activate(shared_gsum, shared_usum, own_squares)
    packing = units_here // shared_units
    stacked = jnp.concatenate(
        [hidden, shared_hidden.reshape(tokens_here // packing, units_here)], axis=0
    )
    columns = local_down.shape[1]
    portion = lax.all_gather(stacked, "tp", axis=1, tiled=True)
    shards_in = portion.shape[1] // units_here
    routed = jnp.dot(portion[:slots_all], local_down, preferred_element_type=jnp.float32)
    shared_piece = portion[slots_all:].reshape(
        tokens_here // packing, shards_in, packing, shared_units
    )
    shared_piece = shared_piece.transpose(0, 2, 1, 3).reshape(tokens_here, shards_in * shared_units)
    shared = jnp.dot(shared_piece, shared_down, preferred_element_type=jnp.float32)
    returned = lax.all_to_all(
        routed.astype(jnp.bfloat16).reshape(ep_size, capacity, columns),
        "ep",
        split_axis=0,
        concat_axis=0,
        tiled=True,
    )
    returned = returned.reshape(slots_all, columns)
    picked = jnp.take(returned, target, axis=0).reshape(tokens_here, TOP_K, columns)
    combined = shared + jnp.sum(route_weights[:, :, None] * picked.astype(jnp.float32), axis=1)
    return (attended, combined.astype(jnp.bfloat16))


def solution(mesh):
    placed = (
        P("ep", "tp"),
        P("ep", "tp"),
        P("ep", "tp"),
        P(),
        P(),
        P("tp"),
        P("ep", "tp"),
        P(),
        P("ep", None),
        P("ep", None),
        P("ep", None, "tp"),
        P("ep", None, "tp"),
        P("ep", None, "tp"),
        P(None, "tp"),
        P(None, "tp"),
        P(None, "tp"),
    )
    return jax.shard_map(
        shards,
        mesh=mesh,
        in_specs=placed,
        out_specs=(P("ep", "tp"), P("ep", "tp")),
        check_vma=False,
    )
```

profile of v0, /device:TPU:1, one launch (start us, length us, event | category | flops | bytes accessed | tf_op | source)
XLA Modules:
  0.0 307.7 jit_solution(4696825488494328392)
XLA Ops:
  8.3 1.5 reduce-window.6
  11.0 4.1 %gather_fusion = bf16[960,256]{1,0:T(8,128)(2,1)S(1)} fusion(bf16[160,256]{1,0:T(8,128)(2,1)S(1)} %copy-done.1, s32[1024]{0:T(1024)S(1)} %pad_clamp_fusion.1), kind=kCustom, calls=%fused_computation | custom fusion | bytes 986880 | tf_op jit(solution)/shard_map/jit(_take)/gather | solution.py:147
  15.7 50.1 %all_to_all.10 = bf16[32,30,256]{2,1,0:T(8,128)(2,1)S(1)} all-to-all(bf16[32,30,256]{2,1,0:T(8,128)(2,1)S(1)} %select_select_fusion), channel_id=1, replica_groups=mesh['ep'=32,'tp'=16] {'ep'}, dimensions={0} | all-to-all | bytes 983040 | tf_op jit(solution)/shard_map/all_to_all | solution.py:149
  66.8 86.5 %all-gather.3.cloned.1.call-done = bf16[1120,4096]{1,0:T(8,128)(2,1)} async-done(((bf16[1120,256]{1,0:T(8,128)(2,1)}), bf16[1120,4096]{1,0:T(8,128)(2,1)}) %all-gather.3.cloned.1.call-update) | async-done | bytes 9175056 | tf_op jit(solution)/shard_map/all_gather | solution.py:33
  153.3 4.8 %fusion.1 = f32[960]{0:T(1024)S(1)} fusion(bf16[1120,4096]{1,0:T(8,128)(2,1)} %all-gather.3.cloned.1.call-done), kind=kLoop, calls=%fused_computation.5 | loop fusion | flops 11795520 | bytes 7868160 | tf_op jit(solution)/shard_map/reduce_sum | solution.py:100
  158.2 1.8 fusion.9
  160.0 1.9 convolution_multiply_fusion.1
  161.8 1.9 fusion.36
  164.0 5.6 %fusion.19 = f32[960,128]{1,0:T(8,128)S(1)} fusion(f32[4096]{0:T(1024)S(1)} %copy-done.18, bf16[1120,4096]{1,0:T(8,128)(2,1)} %all-gather.3.cloned.1.call-done, bf16[1,4096,128]{2,1,0:T(8,128)(2,1)S(1)} %copy-done.14, f32[960]{0:T(1024)S(1)} %add_rsqrt_fusion.1), kind=kOutput, calls=%fused_computation.26 | convolution fusion | flops 1018552320 | bytes 9424640 | tf_op jit(solution)/shard_map/dot_general | solution.py:98
  170.0 2.2 fusion.31
  173.8 2.0 fusion.56
  176.5 5.1 %collective-permute-start = (bf16[2,128,128]{2,1,0:T(8,128)(2,1)}, bf16[2,128,128]{2,1,0:T(8,128)(2,1)}, u32[]{:S(2)}, u32[]{:S(2)}) collective-permute-start(bf16[2,128,128]{2,1,0:T(8,128)(2,1)} %get-tuple-element.19), channel_id=1, source_target_pairs={{0,16},{16,32},{32,48},{48,64},{64,80},{80,96},{96,112},{112,128},... | collective-permute-start | bytes 196616 | tf_op jit(solution)/shard_map/ppermute | solution.py:22
  181.6 2.1 collective-permute-start.1
  188.9 2.4 slice_negate_fusion.1
  191.4 52.9 %all-gather.5.cloned.1.call-done = bf16[1000,2048]{1,0:T(8,128)(2,1)} async-done(((bf16[1000,128]{1,0:T(8,128)(2,1)}), bf16[1000,2048]{1,0:T(8,128)(2,1)}) %all-gather.5.cloned.1.call-update) | async-done | bytes 4096016 | tf_op jit(solution)/shard_map/all_gather | solution.py:170
  244.3 3.3 %fusion.16 = bf16[960,256]{1,0:T(8,128)(2,1)S(1)} fusion(bf16[1000,2048]{1,0:T(8,128)(2,1)} %all-gather.5.cloned.1.call-done, bf16[1,2048,256]{2,1,0:T(8,128)(2,1)S(1)} %copy-done), kind=kOutput, calls=%fused_computation.25 | convolution fusion | flops 1006878720 | bytes 5472256 | tf_op jit(solution)/shard_map/dot_general | solution.py:172
  248.5 14.4 %all-to-all-start.1 = ((bf16[32,30,256]{2,1,0:T(8,128)(2,1)}), bf16[32,30,256]{2,1,0:T(8,128)(2,1)S(1)}, u32[]{:S(2)}, u32[]{:S(2)}) async-start(bf16[32,30,256]{2,1,0:T(8,128)(2,1)} %reshape.420), calls=%async_computation.1 | async-start | bytes 1048576 | tf_op jit(solution)/shard_map/all_to_all | solution.py:178
  262.9 1.4 copy.73
  264.3 1.4 copy.71
  266.5 1.7 fusion.15
  268.1 2.8 maximum_multiply_fusion
  272.7 1.7 fusion.10
  277.7 18.7 %all-to-all-done.1 = bf16[32,30,256]{2,1,0:T(8,128)(2,1)S(1)} async-done(((bf16[32,30,256]{2,1,0:T(8,128)(2,1)}), bf16[32,30,256]{2,1,0:T(8,128)(2,1)S(1)}, u32[]{:S(2)}, u32[]{:S(2)}) %all-to-all-start.1) | async-done | bytes 491552 | tf_op jit(solution)/shard_map/all_to_all | solution.py:178
  296.5 2.8 gather_fusion.1
  (116 shorter events, 20.1 us)
Async XLA Ops:
  7.2 237.1 %copy-start = (bf16[1,2048,256]{2,1,0:T(8,128)(2,1)S(1)}, bf16[1,2048,256]{2,1,0:T(8,128)(2,1)}, u32[]{:S(2)}) copy-start(bf16[1,2048,256]{2,1,0:T(8,128)(2,1)} %param.28) | copy-start | bytes 3145732
  7.2 3.8 %copy-start.1 = (bf16[160,256]{1,0:T(8,128)(2,1)S(1)}, bf16[160,256]{1,0:T(8,128)(2,1)}, u32[]{:S(2)}) copy-start(bf16[160,256]{1,0:T(8,128)(2,1)} %param.22) | copy-start | bytes 245764
  7.2 146.1 %all-gather.3.cloned.1.call-start = ((), (), s32[]{:S(2)}) async-start(), calls=%async_computation.2 | async-start | bytes 9748480 | tf_op jit(solution)/shard_map/all_gather | solution.py:33
  66.8 93.2 %copy-start.16 = (bf16[4096,32]{0,1:T(8,128)(2,1)S(1)}, bf16[4096,32]{0,1:T(8,128)(2,1)}, u32[]{:S(2)}) copy-start(bf16[4096,32]{0,1:T(8,128)(2,1)} %param.29) | copy-start | bytes 786436
  66.8 93.2 %copy-start.18 = (f32[4096]{0:T(1024)S(1)}, f32[4096]{0:T(1024)}, u32[]{:S(2)}) copy-start(f32[4096]{0:T(1024)} %param.23) | copy-start | bytes 49156
  66.8 177.5 %all-gather.5.cloned.1.call-start = ((), (), s32[]{:S(2)}) async-start(), calls=%async_computation.3 | async-start | bytes 4352000 | tf_op jit(solution)/shard_map/all_gather | solution.py:170
  158.1 3.7 %copy-start.17 = (bf16[4096,32]{0,1:T(8,128)(2,1)S(1)}, bf16[4096,32]{0,1:T(8,128)(2,1)}, u32[]{:S(2)}) copy-start(bf16[4096,32]{0,1:T(8,128)(2,1)} %param.30) | copy-start | bytes 786436
  158.2 5.8 %copy-start.14 = (bf16[1,4096,128]{2,1,0:T(8,128)(2,1)S(1)}, bf16[1,4096,128]{2,1,0:T(8,128)(2,1)}, u32[]{:S(2)}) copy-start(bf16[1,4096,128]{2,1,0:T(8,128)(2,1)} %param.26) | copy-start | bytes 3145732
  161.8 7.8 %slice-start = ((s8[9175040]{0:T(1024)(128)(4,1)}), s8[786432]{0:T(1024)(128)(4,1)S(1)}, s32[]{:S(2)}) async-start(s8[9175040]{0:T(1024)(128)(4,1)} %bitcast.125), calls=%async_computation.4 | async-start | bytes 1572864
  164.0 5.7 %slice-start.1 = ((s8[9175040]{0:T(1024)(128)(4,1)}), s8[4194304]{0:T(1024)(128)(4,1)S(1)}, s32[]{:S(2)}) async-start(s8[9175040]{0:T(1024)(128)(4,1)} %bitcast.125), calls=%async_computation.5 | async-start | bytes 8388608
  164.0 6.0 %slice-start.2 = ((s8[9175040]{0:T(1024)(128)(4,1)}), s8[4194304]{0:T(1024)(128)(4,1)S(1)}, s32[]{:S(2)}) async-start(s8[9175040]{0:T(1024)(128)(4,1)} %bitcast.125), calls=%async_computation.6 | async-start | bytes 8388608
  164.0 6.0 %copy-start.15 = (bf16[1,4096,128]{2,1,0:T(8,128)(2,1)S(1)}, bf16[1,4096,128]{2,1,0:T(8,128)(2,1)}, u32[]{:S(2)}) copy-start(bf16[1,4096,128]{2,1,0:T(8,128)(2,1)} %param.27) | copy-start | bytes 3145732
  173.0 10.9 %copy-start.11 = (s32[160,4]{0,1:T(4,128)S(1)}, s32[160,4]{0,1:T(4,128)}, u32[]{:S(2)}) copy-start(s32[160,4]{0,1:T(4,128)} %param.24) | copy-start | bytes 7684
  173.0 11.2 %copy-start.7 = (bf16[512,256]{1,0:T(8,128)(2,1)S(1)}, bf16[512,256]{1,0:T(8,128)(2,1)}, u32[]{:S(2)}) copy-start(bf16[512,256]{1,0:T(8,128)(2,1)} %param.16) | copy-start | bytes 786436
  176.5 94.4 %collective-permute-start = (bf16[2,128,128]{2,1,0:T(8,128)(2,1)}, bf16[2,128,128]{2,1,0:T(8,128)(2,1)}, u32[]{:S(2)}, u32[]{:S(2)}) collective-permute-start(bf16[2,128,128]{2,1,0:T(8,128)(2,1)} %get-tuple-element.19), channel_id=1, source_target_pairs={{0,16},{16,32},{32,48},{48,64},{64,80},{80,96},{96,112},{112,128},... | collective-permute-start | bytes 196616 | tf_op jit(solution)/shard_map/ppermute | solution.py:22
  181.6 89.3 %collective-permute-start.1 = (bf16[2,128,128]{2,1,0:T(8,128)(2,1)}, bf16[2,128,128]{2,1,0:T(8,128)(2,1)}, u32[]{:S(2)}, u32[]{:S(2)}) collective-permute-start(bf16[2,128,128]{2,1,0:T(8,128)(2,1)} %get-tuple-element.20), channel_id=1, source_target_pairs={{16,0},{32,16},{48,32},{64,48},{80,64},{96,80},{112,96},{128,112},... | collective-permute-start | bytes 196616 | tf_op jit(solution)/shard_map/ppermute | solution.py:25
  191.4 75.1 %copy-start.12 = (pred[768]{0:T(1024)(128)(4,1)S(1)}, pred[768]{0:T(1024)(128)(4,1)}, u32[]{:S(2)}) copy-start(pred[768]{0:T(1024)(128)(4,1)} %get-tuple-element.31) | copy-start | bytes 2308
  248.5 47.9 %all-to-all-start.1 = ((bf16[32,30,256]{2,1,0:T(8,128)(2,1)}), bf16[32,30,256]{2,1,0:T(8,128)(2,1)S(1)}, u32[]{:S(2)}, u32[]{:S(2)}) async-start(bf16[32,30,256]{2,1,0:T(8,128)(2,1)} %reshape.420), calls=%async_computation.1 | async-start | bytes 1048576 | tf_op jit(solution)/shard_map/all_to_all | solution.py:178
  265.7 5.2 %copy-start.5 = (bf16[512,128]{1,0:T(8,128)(2,1)S(1)}, bf16[512,128]{1,0:T(8,128)(2,1)}, u32[]{:S(2)}) copy-start(bf16[512,128]{1,0:T(8,128)(2,1)} %param.18) | copy-start | bytes 393220
  265.7 6.2 %copy-start.3 = (f32[512,128]{1,0:T(8,128)S(1)}, f32[512,128]{1,0:T(8,128)}, u32[]{:S(2)}) copy-start(f32[512,128]{1,0:T(8,128)} %get-tuple-element.13) | copy-start | bytes 786436
  265.7 7.0 %copy-start.8 = (bf16[512,256]{1,0:T(8,128)(2,1)S(1)}, bf16[512,256]{1,0:T(8,128)(2,1)}, u32[]{:S(2)}) copy-start(bf16[512,256]{1,0:T(8,128)(2,1)} %param.16) | copy-start | bytes 786436
  276.9 22.5 %copy-start.6 = (f32[160,4]{1,0:T(8,128)S(1)}, f32[160,4]{1,0:T(8,128)}, u32[]{:S(2)}) copy-start(f32[160,4]{1,0:T(8,128)} %copy.71) | copy-start | bytes 7684
  276.9 22.5 %copy-start.10 = (pred[160,4]{1,0:T(8,128)(4,1)S(1)}, pred[160,4]{1,0:T(8,128)(4,1)}, u32[]{:S(2)}) copy-start(pred[160,4]{1,0:T(8,128)(4,1)} %copy.73) | copy-start | bytes 1924
  277.0 23.0 %copy-start.9 = (bf16[512,256]{1,0:T(8,128)(2,1)S(1)}, bf16[512,256]{1,0:T(8,128)(2,1)}, u32[]{:S(2)}) copy-start(bf16[512,256]{1,0:T(8,128)(2,1)} %param.31) | copy-start | bytes 786436
  (4 other events, 11.7 us)
Sparse Core Ops, SparseCore 0:
  66.9 86.3 all-gather.2
  173.1 71.1 all-gather.4
where the time goes:
time: 308 us
  waiting for transfers between devices  158 us (51%)
  blocking collectives  50.1 us (16%)
  other arithmetic  25.9 us (8%)
  starting transfers between devices  21.6 us (7%)
  local copies, waits for them, and re-layouts  18.7 us (6%)
  matrix products  18.6 us (6%)
  between operations  14.7 us (5%)
    all_gather x1, waiting for transfers between devices, side_by_side(): whole = lax.all_gather(both, axis, axis=dim, tiled=True)  86.5 us
    all_gather x1, waiting for transfers between devices, shards(): portion = lax.all_gather(stacked, 'tp', axis=1, tiled=True)  52.9 us
    all_to_all x1, blocking collectives, shards(): lax.all_to_all(outgoing.reshape(ep_size, capacity, width_here), 'ep', spl...  50.1 us
    all_to_all x1, waiting for transfers between devices, shards(): lax.all_to_all(routed.astype(jnp.bfloat16).reshape(ep_size, capacity, col...  18.7 us
    all_to_all x1, starting transfers between devices, shards(): lax.all_to_all(routed.astype(jnp.bfloat16).reshape(ep_size, capacity, col...  14.4 us
    dot_general x2, matrix products, project(): gate_sum = jnp.dot(weighted, gate_rows, preferred_element_type=jnp.float32)  7.46 us
    reduce_sum x2, other arithmetic, project(): return (gate_sum, up_sum, jnp.sum(floats * floats, axis=1))  6.59 us
  transfers between devices with their start and end apart: 5, of which 3 were waited for; matrix products, arithmetic and copies ran while one was open for 10% of the time, Pallas kernels for 0%

commit v1 on v0

v1 whole, which is shorter than its diff:
```python
import numpy as np
import jax
import jax.numpy as jnp
from jax import lax
from jax.experimental import pallas as pl
from jax.experimental.pallas import tpu as pltpu
from jax.sharding import PartitionSpec as P

MESH = pl.DeviceIdType.MESH
BF = jnp.bfloat16
F32 = jnp.float32

HEAD_DIM = 128
WINDOW = 128
GRID_W = 64
D = 4096
TOP_K = 4
EPS = 1e-06
ROTARY_BASE = 10000.0

NZ = 16
TOK = 160
TPAD = 256
SLOT = 32
ROWS = 32 * SLOT
LEN = 512
FEAT = 256
UNITS = 128
PACK = 64

REL = [0, 1, -1, 8, 7, -7, 6, -6, 5, -5, 4, -4, 3, -3, 2, -2]


def _inv(p):
    return REL.index(REL[p] if REL[p] in (0, 8) else -REL[p])


INV = [_inv(p) for p in range(NZ)]
CHUNK = 256
NCHUNK = ROWS // CHUNK

GATHER_1 = [(c * CHUNK, CHUNK) for c in range(NCHUNK)] + [(ROWS, TOK)]
GATHER_2 = [(c * CHUNK, CHUNK) for c in range(NCHUNK)] + [(ROWS, PACK)]
OWN = NCHUNK


def up16(v):
    return (v + 15) // 16 * 16


def kernel(
    x_ref,
    ids_ref,
    rw_ref,
    q_ref,
    k_ref,
    v_ref,
    qg_ref,
    kg_ref,
    sink_ref,
    ng_ref,
    colt_ref,
    rowt_hbm,
    gate_hbm,
    up_hbm,
    down_hbm,
    sg_ref,
    su_ref,
    sd_hbm,
    att_ref,
    out_ref,
    xg,
    hg,
    wgu,
    wd,
    wsd,
    rowt,
    kpad,
    vpad,
    qt,
    kt,
    xpad,
    idsp,
    rwp,
    send,
    wt_hi,
    wt_lo,
    lhs,
    res,
    ret,
    acc,
    sh_acc,
    bar_dummy,
    g_send,
    g_recv,
    zi_send,
    zi_recv,
    zo_send,
    zo_recv,
    halo_send,
    halo_recv,
    loc,
):
    ep = lax.axis_index("ep")
    tp = lax.axis_index("tp")
    z = ep // 2
    core = ep % 2
    y = tp // 4
    x = tp % 4
    xr, xl = (x + 1) % 4, (x + 3) % 4
    yr, yl = (y + 1) % 4, (y + 3) % 4

    def ep_at(rel, c):
        return ((z + rel + NZ) % NZ) * 2 + c

    ep_hi = (ep + 1) % 32
    ep_lo = (ep + 31) % 32

    barrier = pltpu.get_barrier_semaphore()
    for p in range(NZ):
        for c in range(2):
            if p == 0:
                continue
            pl.semaphore_signal(
                barrier, inc=1, device_id={"ep": ep_at(REL[p], c), "tp": tp}, device_id_type=MESH
            )
    pl.semaphore_signal(
        barrier, inc=1, device_id={"ep": z * 2 + (1 - core), "tp": tp}, device_id_type=MESH
    )
    plane = [y * 4 + xr, y * 4 + xl, yr * 4 + x, yl * 4 + x]
    for t in plane:
        pl.semaphore_signal(barrier, inc=1, device_id={"ep": ep, "tp": t}, device_id_type=MESH)

    loads = [
        pltpu.make_async_copy(gate_hbm.at[0], wgu.at[:, 0:128], loc.at[0]),
        pltpu.make_async_copy(up_hbm.at[0], wgu.at[:, 128:256], loc.at[1]),
        pltpu.make_async_copy(down_hbm.at[0], wd, loc.at[2]),
        pltpu.make_async_copy(
            rowt_hbm.at[:, pl.ds(pl.multiple_of(ep * 8, 8), 16), :], rowt, loc.at[3]
        ),
    ] + [
        pltpu.make_async_copy(sd_hbm, wsd.at[:, pl.ds(32 * j, 32), :], loc.at[4 + j])
        for j in range(4)
    ]
    for cp in loads:
        cp.start()

    xg[y, x, ROWS : ROWS + TOK, :] = x_ref[...]
    xpad[...] = jnp.zeros_like(xpad)
    xpad[0:TOK, :] = x_ref[...]
    idsp[...] = jnp.full(idsp.shape, -1, jnp.int32)
    idsp[0:TOP_K, 0:TOK] = ids_ref[...]
    rwp[...] = jnp.zeros_like(rwp)
    rwp[0:TOP_K, 0:TOK] = rw_ref[...]
    kpad[WINDOW : WINDOW + LEN, :] = k_ref[...]
    vpad[WINDOW : WINDOW + LEN, :] = v_ref[...]

    row32 = lax.broadcasted_iota(jnp.int32, (32, TPAD), 0)
    pos32 = row32 >> 1
    rel32 = jnp.zeros((32, TPAD), jnp.int32)
    for p in range(NZ):
        rel32 = jnp.where(pos32 == p, REL[p] + NZ, rel32)
    expert32 = ((z + rel32) & (NZ - 1)) * 2 + (row32 & 1)
    named = jnp.zeros((32, TPAD), F32)
    weight = jnp.zeros((32, TPAD), F32)
    for k in range(TOP_K):
        same = idsp[k : k + 1, :] == expert32
        named = jnp.where(same, 1.0, named)
        weight = jnp.where(same, rwp[k : k + 1, :], weight)
    before = (
        lax.broadcasted_iota(jnp.int32, (TPAD, TPAD), 0)
        < lax.broadcasted_iota(jnp.int32, (TPAD, TPAD), 1)
    )
    count = jnp.dot(
        named.astype(BF), jnp.where(before, 1.0, 0.0).astype(BF), preferred_element_type=F32
    )
    slot32 = jnp.where(named > 0.5, count, -1.0)
    slot_row = lax.broadcasted_iota(jnp.int32, (SLOT, TPAD), 0).astype(F32)
    for t in range(NCHUNK):
        picks = [
            jnp.where(slot32[i : i + 1, :] == slot_row, 1.0, 0.0).astype(BF)
            for i in range(8 * t, 8 * t + 8)
        ]
        send[CHUNK * t : CHUNK * (t + 1), :] = jnp.dot(
            jnp.concatenate(picks, axis=0), xpad[...], preferred_element_type=F32
        ).astype(BF)
    xg[y, x, pl.ds(pl.multiple_of(core * SLOT, SLOT), SLOT), :] = send[
        pl.ds(pl.multiple_of(core * SLOT, SLOT), SLOT), :
    ]

    pl.semaphore_wait(barrier, 35)

    sends = []

    def remote(src, dst, ssem, rsem, dev):
        cp = pltpu.make_async_remote_copy(
            src_ref=src,
            dst_ref=dst,
            send_sem=ssem,
            recv_sem=rsem,
            device_id=dev,
            device_id_type=MESH,
        )
        sends.append(cp)
        return cp

    class Gather:
        def __init__(self, which, buf, start, size, index):
            self.buf, self.index, self.which = buf, index, which
            na = up16(size // 2)
            self.ranges = []
            for first, count in ((start, na), (start + na, size - na)):
                low = up16(count // 2)
                self.ranges.append((first, count, low))
            self.stage = 0
            self.pending = []

        def next(self):
            for cp in self.pending:
                cp.wait_recv()
            self.pending = []
            s = self.stage
            self.stage += 1
            if s == 4:
                return
            buf = self.buf
            for half, (first, count, low) in enumerate(self.ranges):
                full = pl.ds(first, count)
                part_lo, part_hi = pl.ds(first, low), pl.ds(first + low, count - low)
                if half == 0:
                    near = lambda v, r: buf.at[y, v, r]
                    wide = lambda v, r: buf.at[v, :, r]
                    n_me, n_r, n_l, w_me, w_r, w_l = x, xr, xl, y, yr, yl
                    to_nr, to_nl = y * 4 + xr, y * 4 + xl
                    to_wr, to_wl = yr * 4 + x, yl * 4 + x
                else:
                    near = lambda v, r: buf.at[v, x, r]
                    wide = lambda v, r: buf.at[:, v, r]
                    n_me, n_r, n_l, w_me, w_r, w_l = y, yr, yl, x, xr, xl
                    to_nr, to_nl = yr * 4 + x, yl * 4 + x
                    to_wr, to_wl = y * 4 + xr, y * 4 + xl
                if s == 0:
                    pair = ((near(n_me, full), to_nr), (near(n_me, full), to_nl))
                elif s == 1:
                    pair = ((near(n_l, part_lo), to_nr), (near(n_r, part_hi), to_nl))
                elif s == 2:
                    pair = ((wide(w_me, full), to_wr), (wide(w_me, full), to_wl))
                else:
                    pair = ((wide(w_l, part_lo), to_wr), (wide(w_r, part_hi), to_wl))
                for direction, (ref, to) in enumerate(pair):
                    i = ((self.which * 5 + self.index) * 2 + half) * 8 + s * 2 + direction
                    cp = remote(ref, ref, g_send.at[i], g_recv.at[i], {"ep": ep, "tp": to})
                    cp.start()
                    self.pending.append(cp)

    rows_g = [Gather(0, xg, s, n, i) for i, (s, n) in enumerate(GATHER_1)]
    hid_g = [Gather(1, hg, s, n, i) for i, (s, n) in enumerate(GATHER_2)]

    zin = {}

    def start_zin(p):
        for c in range(2):
            if p == 0:
                if c == 1:
                    continue
                c = 1 - core
            src = send.at[pl.ds(pl.multiple_of(p * 2 * SLOT + c * SLOT, SLOT), SLOT)]
            q = INV[p]
            dst = xg.at[y, x, pl.ds(pl.multiple_of(q * 2 * SLOT + core * SLOT, SLOT), SLOT)]
            cp = remote(
                src,
                dst,
                zi_send.at[2 * p + c],
                zi_recv.at[2 * q + core],
                {"ep": ep_at(REL[p], c), "tp": tp},
            )
            cp.start()

    def wait_block(buf_at, recv, p):
        for c in range(2):
            if p == 0:
                if c == 1:
                    continue
                c = 1 - core
            dst = buf_at(pl.ds(pl.multiple_of(p * 2 * SLOT + c * SLOT, SLOT), SLOT))
            pltpu.make_async_remote_copy(
                src_ref=dst,
                dst_ref=dst,
                send_sem=zi_send.at[0],
                recv_sem=recv.at[2 * p + c],
                device_id={"ep": z * 2 + (1 - core), "tp": tp},
                device_id_type=MESH,
            ).wait_recv()

    def wait_zin(chunk):
        for p in range(4 * chunk, 4 * chunk + 4):
            wait_block(lambda r: xg.at[y, x, r], zi_recv, p)

    def start_zout(chunk):
        for p in range(4 * chunk, 4 * chunk + 4):
            q = INV[p]
            for c in range(2):
                if p == 0:
                    if c == 1:
                        continue
                    c = 1 - core
                src = res.at[pl.ds(pl.multiple_of(p * 2 * SLOT + c * SLOT, SLOT), SLOT)]
                dst = ret.at[pl.ds(pl.multiple_of(q * 2 * SLOT + core * SLOT, SLOT), SLOT)]
                cp = remote(
                    src,
                    dst,
                    zo_send.at[2 * p + c],
                    zo_recv.at[2 * q + core],
                    {"ep": ep_at(REL[p], c), "tp": tp},
                )
                cp.start()

    def wait_zout(chunk):
        for p in range(4 * chunk, 4 * chunk + 4):
            wait_block(lambda r: ret.at[r], zo_recv, p)

    halos = []

    def start_halo():
        tail, head = pl.ds(LEN - WINDOW, WINDOW), pl.ds(0, WINDOW)
        for i, (ref, pad) in enumerate(((k_ref, kpad), (v_ref, vpad))):
            for j, (part, to, at) in enumerate(
                ((tail, ep_hi, head), (head, ep_lo, pl.ds(WINDOW + LEN, WINDOW)))
            ):
                cp = remote(
                    ref.at[part],
                    pad.at[at],
                    halo_send.at[2 * i + j],
                    halo_recv.at[2 * i + j],
                    {"ep": to, "tp": tp},
                )
                cp.start()
                halos.append(cp)

    first_half = (lax.broadcasted_iota(jnp.int32, (GRID_W, HEAD_DIM), 1) & 63) < 32

    def turn(raw, gain, g):
        f = raw.astype(F32)
        n = f * lax.rsqrt(jnp.mean(f * f, axis=-1, keepdims=True) + EPS) * gain
        other = jnp.where(first_half, pltpu.roll(n, 96, 1), pltpu.roll(n, 32, 1))
        cos = rowt[0, pl.ds(g, 1), :] + colt_ref[0]
        sin = rowt[1, pl.ds(g, 1), :] + colt_ref[1]
        return (n * cos + other * sin).astype(BF)

    def turn_queries():
        for g in range(LEN // GRID_W):
            for h in range(2):
                rows = slice(g * GRID_W, (g + 1) * GRID_W)
                qt[h, rows, :] = turn(
                    q_ref[rows, h * HEAD_DIM : (h + 1) * HEAD_DIM], qg_ref[...], g + 2
                )

    def turn_keys():
        for g in range((LEN + 2 * WINDOW) // GRID_W):
            rows = slice(g * GRID_W, (g + 1) * GRID_W)
            kt[rows, :] = turn(kpad[rows, :], kg_ref[...], g)

    near_q = lax.broadcasted_iota(jnp.int32, (128, 384), 0)
    near_k = lax.broadcasted_iota(jnp.int32, (128, 384), 1)

    def attend(b):
        key_pos = near_k + (ep * LEN - WINDOW + 128 * b)
        inside = (
            (near_k >= near_q)
            & (near_k <= near_q + 2 * WINDOW)
            & (key_pos >= 0)
            & (key_pos < 32 * LEN)
        )
        keys = kt[128 * b : 128 * b + 384, :]
        values = vpad[128 * b : 128 * b + 384, :]
        for h in range(2):
            scores = lax.dot_general(
                qt[h, 128 * b : 128 * b + 128, :],
                keys,
                (((1,), (1,)), ((), ())),
                preferred_element_type=F32,
            ) * (HEAD_DIM ** (-0.5))
            raised = jnp.where(inside, jnp.exp(scores), 0.0)
            sink = jnp.exp(jnp.full((128, 1), sink_ref[h], F32))
            den = sink + jnp.sum(raised, axis=-1, keepdims=True)
            weights = (raised * (1.0 / den)).astype(BF)
            mixed = jnp.dot(weights, values, preferred_element_type=F32)
            att_ref[128 * b : 128 * b + 128, h * 128 : (h + 1) * 128] = mixed.astype(BF)

    def scale_rows(start, size):
        acc[0:size, 0:128] = jnp.zeros((size, 128), F32)

        def one(s, carry):
            f = xg[s // 4, s % 4, start : start + size, :].astype(F32)
            sq = f * f
            acc[0:size, 0:128] += sq[:, 0:128] + sq[:, 128:256]
            lhs[s, 0:size, :] = (f * ng_ref[pl.ds(s, 1), :]).astype(BF)
            return carry

        lax.fori_loop(0, 16, one, 0)
        return lax.rsqrt(jnp.sum(acc[0:size, 0:128], axis=-1, keepdims=True) / D + EPS)

    def activate(g, u, factor):
        g, u = g * factor, u * factor
        return (g / (1.0 + jnp.exp(-g)) * u).astype(BF)

    def experts_in(c):
        start = c * CHUNK
        factor = scale_rows(start, CHUNK)
        both = jnp.dot(
            jnp.concatenate([lhs[s] for s in range(16)], axis=1),
            wgu[...],
            preferred_element_type=F32,
        )
        hg[y, x, start : start + CHUNK, :] = activate(both[:, 0:128], both[:, 128:256], factor)

    def shared_in():
        factor = scale_rows(ROWS, TOK)
        rows = jnp.concatenate([lhs[s, 0:TOK, :] for s in range(16)], axis=1)
        g = jnp.dot(rows, sg_ref[...], preferred_element_type=F32)
        u = jnp.dot(rows, su_ref[...], preferred_element_type=F32)
        h = activate(g, u, factor).astype(F32)
        packed = jnp.concatenate([h[40 * j : 40 * j + 40, :] for j in range(4)], axis=1)
        packed = jnp.concatenate([packed, jnp.zeros((PACK - 40, 128), F32)], axis=0)
        hg[y, x, ROWS : ROWS + PACK, :] = packed.astype(BF)

    def experts_out(c):
        start = c * CHUNK
        rows = jnp.concatenate(
            [hg[s // 4, s % 4, start : start + CHUNK, :] for s in range(16)], axis=1
        )
        res[start : start + CHUNK, :] = jnp.dot(
            rows, wd[...], preferred_element_type=F32
        ).astype(BF)
        if c == 0:
            mine = pl.ds(pl.multiple_of(core * SLOT, SLOT), SLOT)
            ret[mine, :] = res[mine, :]

    def shared_out():
        group = lax.broadcasted_iota(jnp.int32, (40, 128), 1) // 32
        total = jnp.zeros((TOK, FEAT), F32)
        for s in range(16):
            piece = hg[s // 4, s % 4, ROWS : ROWS + PACK, :].astype(F32)[0:40, :]
            parts = jnp.concatenate(
                [jnp.where(group == j, piece, 0.0) for j in range(4)], axis=0
            )
            total += jnp.dot(parts.astype(BF), wsd[s], preferred_element_type=F32)
        sh_acc[...] = total

    def combine_weights():
        for t in range(NCHUNK):
            full = jnp.concatenate(
                [
                    jnp.where(slot32[i : i + 1, :] == slot_row, weight[i : i + 1, :], 0.0)
                    for i in range(8 * t, 8 * t + 8)
                ],
                axis=0,
            )
            turned = jnp.transpose(full)
            high = turned.astype(BF)
            wt_hi[t] = high
            wt_lo[t] = (turned - high.astype(F32)).astype(BF)

    def combine(c):
        rows = ret[c * CHUNK : (c + 1) * CHUNK, :]
        part = jnp.dot(wt_hi[c], rows, preferred_element_type=F32) + jnp.dot(
            wt_lo[c], rows, preferred_element_type=F32
        )
        sh_acc[...] += part[0:TOK, :]

    R1, R2, R3, R4, O1 = rows_g
    H1, H2, H3, H4, S2 = hid_g

    O1.next()
    for p in range(NZ):
        start_zin(p)
    start_halo()
    combine_weights()
    for cp in loads[3:]:
        cp.wait()
    O1.next()
    wait_zin(0)
    R1.next()
    O1.next()
    turn_queries()
    R1.next()
    O1.next()
    wait_zin(1)
    R2.next()
    R1.next()
    for cp in halos:
        cp.wait_recv()
    turn_keys()
    O1.next()
    R2.next()
    shared_in()
    S2.next()
    R1.next()
    attend(0)
    S2.next()
    wait_zin(2)
    R3.next()
    R2.next()
    attend(1)
    S2.next()
    R1.next()
    for cp in loads[:3]:
        cp.wait()
    experts_in(0)
    H1.next()
    R3.next()
    R2.next()
    S2.next()
    H1.next()
    wait_zin(3)
    R4.next()
    R3.next()
    attend(2)
    R2.next()
    experts_in(1)
    H2.next()
    H1.next()
    R4.next()
    R3.next()
    H2.next()
    S2.next()
    shared_out()
    R4.next()
    attend(3)
    R3.next()
    experts_in(2)
    H3.next()
    H1.next()
    H2.next()
    R4.next()
    H3.next()
    H1.next()
    experts_out(0)
    start_zout(0)
    H2.next()
    H3.next()
    R4.next()
    experts_in(3)
    H4.next()
    H2.next()
    experts_out(1)
    start_zout(1)
    H3.next()
    H4.next()
    wait_zout(0)
    combine(0)
    H4.next()
    H3.next()
    experts_out(2)
    start_zout(2)
    H4.next()
    wait_zout(1)
    combine(1)
    H4.next()
    experts_out(3)
    start_zout(3)
    wait_zout(2)
    combine(2)
    wait_zout(3)
    combine(3)
    out_ref[...] = sh_acc[...].astype(BF)
    for cp in sends:
        cp.wait_send()


def _tables():
    quarter = HEAD_DIM // 4
    freq = np.float32(ROTARY_BASE) ** (
        np.float32(-4.0) * np.arange(quarter, dtype=np.float32) / np.float32(HEAD_DIM)
    )
    freq = freq.astype(np.float32)
    sign = np.concatenate([-np.ones(quarter), np.ones(quarter)])

    def of(index):
        angle = (index.astype(np.float32)[:, None] * freq).astype(np.float32).astype(np.float64)
        angle = np.concatenate([angle, angle], axis=1)
        return np.cos(angle), np.sin(angle) * sign

    def put(pair, left):
        pads = [(0, 0), (0, 64)] if left else [(0, 0), (64, 0)]
        return np.stack([np.pad(v, pads) for v in pair]).astype(np.float32)

    rows = put(of(np.arange(-2, 270)), True)
    cols = put(of(np.arange(GRID_W)), False)
    return rows, cols


ROW_TABLE, COL_TABLE = _tables()


def shards(
    query_vectors,
    key_vectors,
    value_vectors,
    query_gain,
    key_gain,
    sink_logits,
    moe_rows,
    norm_gain,
    expert_ids,
    route_weights,
    expert_gate,
    expert_up,
    expert_down,
    shared_gate,
    shared_up,
    shared_down,
):
    vm = pl.BlockSpec(memory_space=pltpu.VMEM)
    sm = pl.BlockSpec(memory_space=pltpu.SMEM)
    hb = pl.BlockSpec(memory_space=pl.ANY)
    dma = pltpu.SemaphoreType.DMA
    return pl.pallas_call(
        kernel,
        out_shape=(
            jax.ShapeDtypeStruct((LEN, 2 * HEAD_DIM), BF),
            jax.ShapeDtypeStruct((TOK, FEAT), BF),
        ),
        in_specs=[vm] * 8 + [sm] + [vm] * 2 + [hb] * 4 + [vm] * 2 + [hb],
        out_specs=(vm, vm),
        scratch_shapes=[
            pltpu.VMEM((4, 4, ROWS + TOK, FEAT), BF),
            pltpu.VMEM((4, 4, ROWS + PACK, UNITS), BF),
            pltpu.VMEM((D, 2 * UNITS), BF),
            pltpu.VMEM((16 * UNITS, FEAT), BF),
            pltpu.VMEM((16, 128, FEAT), BF),
            pltpu.VMEM((2, 16, 128), F32),
            pltpu.VMEM((LEN + 2 * WINDOW, HEAD_DIM), BF),
            pltpu.VMEM((LEN + 2 * WINDOW, HEAD_DIM), BF),
            pltpu.VMEM((2, LEN, HEAD_DIM), BF),
            pltpu.VMEM((LEN + 2 * WINDOW, HEAD_DIM), BF),
            pltpu.VMEM((TPAD, FEAT), BF),
            pltpu.VMEM((8, TPAD), jnp.int32),
            pltpu.VMEM((8, TPAD), F32),
            pltpu.VMEM((ROWS, FEAT), BF),
            pltpu.VMEM((NCHUNK, TPAD, CHUNK), BF),
            pltpu.VMEM((NCHUNK, TPAD, CHUNK), BF),
            pltpu.VMEM((16, CHUNK, FEAT), BF),
            pltpu.VMEM((ROWS, FEAT), BF),
            pltpu.VMEM((ROWS, FEAT), BF),
            pltpu.VMEM((CHUNK, 128), F32),
            pltpu.VMEM((TOK, FEAT), F32),
            pltpu.SMEM((1,), jnp.int32),
            dma((160,)),
            dma((160,)),
            dma((32,)),
            dma((32,)),
            dma((32,)),
            dma((32,)),
            dma((4,)),
            dma((4,)),
            dma((8,)),
        ],
        compiler_params=pltpu.CompilerParams(
            collective_id=0, has_side_effects=True, vmem_limit_bytes=50 * 1024 * 1024
        ),
        name="fused",
    )(
        moe_rows,
        expert_ids.T,
        route_weights.T,
        query_vectors,
        key_vectors,
        value_vectors,
        query_gain.reshape(1, HEAD_DIM),
        key_gain.reshape(1, HEAD_DIM),
        sink_logits,
        norm_gain.reshape(16, FEAT),
        jnp.asarray(COL_TABLE),
        jnp.asarray(ROW_TABLE),
        expert_gate,
        expert_up,
        expert_down,
        shared_gate,
        shared_up,
        shared_down.reshape(16, 32, FEAT),
    )


def solution(mesh):
    placed = (
        P("ep", "tp"),
        P("ep", "tp"),
        P("ep", "tp"),
        P(),
        P(),
        P("tp"),
        P("ep", "tp"),
        P(),
        P("ep", None),
        P("ep", None),
        P("ep", None, "tp"),
        P("ep", None, "tp"),
        P("ep", None, "tp"),
        P(None, "tp"),
        P(None, "tp"),
        P(None, "tp"),
    )
    return jax.shard_map(
        shards,
        mesh=mesh,
        in_specs=placed,
        out_specs=(P("ep", "tp"), P("ep", "tp")),
        check_vma=False,
    )
```

time: 308 us -> 141 us (0.46)
  waiting for transfers between devices: 158 us -> 0 us
  Pallas kernels: 0 us -> 129 us
  blocking collectives: 50.1 us -> 0 us
  other arithmetic: 25.9 us -> 0 us
  starting transfers between devices: 21.6 us -> 0 us
  matrix products: 18.6 us -> 0 us
  between operations: 14.7 us -> 0.74 us
  local copies, waits for them, and re-layouts: 18.7 us -> 11.4 us
    all_gather x2 -> x0, waiting for transfers between devices: 139 us -> none  [the longest x1 86.5 us: side_by_side(): whole = lax.all_gather(both, axis, axis=dim, tiled=True)]
    pallas_call x0 -> x1, Pallas kernels: none -> 129 us  [shards(): pl.pallas_call(kernel, out_shape=(jax.ShapeDtypeStruct((LEN, 2 * HEAD_DIM...]
    all_to_all x1 -> x0, blocking collectives: 50.1 us -> none  [shards(): lax.all_to_all(outgoing.reshape(ep_size, capacity, width_here), 'ep', spl...]
    all_to_all x1 -> x0, waiting for transfers between devices: 18.7 us -> none  [shards(): lax.all_to_all(routed.astype(jnp.bfloat16).reshape(ep_size, capacity, col...]
    dot_general x8 -> x0, matrix products: 18.6 us -> none  [the longest x2 7.46 us: project(): gate_sum = jnp.dot(weighted, gate_rows, preferred_element_type=jnp.float32)]
    all_to_all x1 -> x0, starting transfers between devices: 14.4 us -> none  [shards(): lax.all_to_all(routed.astype(jnp.bfloat16).reshape(ep_size, capacity, col...]
    reduce_sum x7 -> x0, other arithmetic: 8.36 us -> none  [the longest x2 6.59 us: project(): return (gate_sum, up_sum, jnp.sum(floats * floats, axis=1))]
    ppermute x2 -> x0, starting transfers between devices: 7.2 us -> none  [the longest x1 5.09 us: padded_2(): lax.ppermute(lax.slice_in_dim(block, block.shape[dim] - width, None, axis...]
  transfers between devices with their start and end apart: 5 -> 0, of which waited for: 3 -> 0; matrix products, arithmetic and copies ran while one was open for 10% -> 0% of each run, Pallas kernels for 0% -> 0%
where the time goes in v1:
time: 141 us
  Pallas kernels  129 us (91%)
  local copies, waits for them, and re-layouts  11.4 us (8%)
    pallas_call x1, Pallas kernels, shards(): pl.pallas_call(kernel, out_shape=(jax.ShapeDtypeStruct((LEN, 2 * HEAD_DIM...  129 us
    unnamed x32, local copies, waits for them, and re-layouts  10.6 us

profile of v1, /device:TPU:1, one launch (start us, length us, event | category | flops | bytes accessed | tf_op | source)
XLA Modules:
  0.0 141.0 jit_solution(889475963676609954)
XLA Ops:
  0.6 0.0 copy-start.3
  0.6 0.8 reshape.18.ng_ref
  1.4 2.4 %copy.20.sg_ref = bf16[4096,32]{1,0:T(8,128)(2,1)} copy(bf16[4096,32]{0,1:T(8,128)(2,1)} %param.31) | data formatting | bytes 524288 | tf_op args[13]
  3.9 0.0 copy-start.12
  3.9 0.0 copy-start.13
  3.9 2.3 %copy.21.su_ref = bf16[4096,32]{1,0:T(8,128)(2,1)} copy(bf16[4096,32]{0,1:T(8,128)(2,1)} %param.32) | data formatting | bytes 524288 | tf_op args[14]
  6.2 0.0 copy-done.3
  6.2 0.0 copy-done
  6.2 0.0 copy-done.1
  6.2 0.0 copy-done.2
  6.2 0.0 copy-done.9
  6.2 0.0 copy-done.10
  6.2 0.0 copy-done.11
  6.3 0.0 copy-done.12
  6.3 0.0 copy-done.13
  6.3 0.0 copy-start.4
  6.3 0.9 copy-done.4
  7.2 0.9 copy-done.5
  8.1 0.9 copy-done.6
  9.0 0.9 copy-done.7
  9.9 0.8 copy-done.8
  10.8 128.9 %fused.1 = (bf16[512,256]{1,0:T(8,128)(2,1)S(1)}, bf16[160,256]{1,0:T(8,128)(2,1)S(1)}) custom-call(bf16[160,256]{1,0:T(8,128)(2,1)S(1)} %copy-done.7, s32[4,160]{1,0:T(4,128)S(1)} %bitcast.6, f32[4,160]{1,0:T(4,128)S(1)} %bitcast.7, bf16[512,256]{1,0:T(8,128)(2,1)S(1)} %copy-done.3, bf16[512,128]{1,0:T(8,128)(2,1)S(1)} %copy-done.5, ...), custom_call_target="tpu_custom_call" | custom-call | tf_op jit(solution)/shard_map/fused/pallas_call | solution.py:618
  139.7 0.7 copy.24
  140.4 0.6 copy.25
  (10 shorter events, 0.0 us)
Async XLA Ops:
  0.6 5.6 %copy-start.3 = (bf16[512,256]{1,0:T(8,128)(2,1)S(1)}, bf16[512,256]{1,0:T(8,128)(2,1)}, u32[]{:S(2)}) copy-start(bf16[512,256]{1,0:T(8,128)(2,1)} %q_ref.1) | copy-start | bytes 786436
  1.4 4.8 %copy-start = (bf16[1,4096,128]{2,1,0:T(8,128)(2,1)S(1)}, bf16[1,4096,128]{2,1,0:T(8,128)(2,1)}, u32[]{:S(2)}) copy-start(bf16[1,4096,128]{2,1,0:T(8,128)(2,1)} %gate_hbm.1) | copy-start | bytes 3145732
  1.4 4.8 %copy-start.1 = (bf16[1,4096,128]{2,1,0:T(8,128)(2,1)S(1)}, bf16[1,4096,128]{2,1,0:T(8,128)(2,1)}, u32[]{:S(2)}) copy-start(bf16[1,4096,128]{2,1,0:T(8,128)(2,1)} %up_hbm.1) | copy-start | bytes 3145732
  3.8 2.4 %copy-start.2 = (f32[2,272,128]{2,1,0:T(8,128)S(1)}, f32[2,272,128]{2,1,0:T(8,128)}, u32[]{:S(2)}) copy-start(f32[2,272,128]{2,1,0:T(8,128)} %constant.5.clone.rowt_hbm) | copy-start | bytes 835588
  3.8 2.4 %copy-start.9 = (s32[160,4]{0,1:T(4,128)S(1)}, s32[160,4]{0,1:T(4,128)}, u32[]{:S(2)}) copy-start(s32[160,4]{0,1:T(4,128)} %param.26) | copy-start | bytes 7684
  3.8 2.4 %copy-start.10 = (f32[160,4]{0,1:T(4,128)S(1)}, f32[160,4]{0,1:T(4,128)}, u32[]{:S(2)}) copy-start(f32[160,4]{0,1:T(4,128)} %param.27) | copy-start | bytes 7684
  3.8 2.4 %copy-start.11 = (f32[128]{0:T(128)S(1)}, f32[128]{0:T(128)}, u32[]{:S(2)}) copy-start(f32[128]{0:T(128)} %param.21) | copy-start | bytes 1540
  3.9 2.4 %copy-start.12 = (f32[128]{0:T(128)S(1)}, f32[128]{0:T(128)}, u32[]{:S(2)}) copy-start(f32[128]{0:T(128)} %param.22) | copy-start | bytes 1540
  3.9 2.4 %copy-start.13 = (f32[2]{0:T(128)S(1)}, f32[2]{0:T(128)}, u32[]{:S(2)}) copy-start(f32[2]{0:T(128)} %sink_ref.1) | copy-start | bytes 28
  6.3 1.0 copy-start.4
  7.2 0.9 copy-start.5
  8.1 0.9 copy-start.6
  9.0 0.9 copy-start.7
  9.9 0.8 copy-start.8
